TPU v7x, 32 devices: a whole 2x2x4 slice. The times are simulated.
32 devices in a mesh: sp: 8 (over z, x), tp: 4 (over y, core).
Axes of the slice: x: 2, y: 2, z: 4, core: 2. Of those that a mesh axis runs over, the one named last changes fastest.
Arguments:
- inputs: bfloat16 [4096, 2048], P('sp', 'tp'), may hold values from -45 to 45
- norm_gain: float32 [3, 2048], replicated, may hold values from 0.1 to 1.9
- w_value: bfloat16 [3, 2048, 1024], P(None, 'sp', 'tp'), may hold values from -0.125 to 0.125
- w_gate: bfloat16 [3, 2048, 1024], P(None, 'sp', 'tp'), may hold values from -0.125 to 0.125
- conv_taps: float32 [3, 31, 1024], P(None, None, 'tp'), may hold values from -5 to 5
- ln_gain: float32 [3, 1024], P(None, 'tp'), may hold values from 0.1 to 1.9
- ln_bias: float32 [3, 1024], P(None, 'tp'), may hold values from -3 to 3
- w_out: bfloat16 [3, 1024, 2048], P(None, 'tp', 'sp'), may hold values from -0.1875 to 0.1875
Outputs:
- stream: bfloat16 [4096, 2048], P('sp', 'tp')
All inputs are finite; a program needn't handle non-finite values.
Results may differ from a plain program's by a relative error of at most 0.01.
Values may be sent and summed in bfloat16 or wider, within the bound.
A program may use at most 64 MiB of HBM per device.

v0:
```python
import jax
import jax.numpy as jnp
from jax import lax
from jax.sharding import PartitionSpec as P


def from_behind(block, axis, distance):
    devices = range(lax.axis_size(axis))
    route = [(i - distance, i) for i in devices if i - distance in devices]
    return lax.ppermute(block, axis, route)


def shards(inputs, norm_gain, w_value, w_gate, conv_taps, ln_gain, ln_bias, w_out):
    rows = inputs.shape[0]
    reach = conv_taps.shape[1] - 1
    layers = conv_taps.shape[0]
    channels = conv_taps.shape[2] * lax.axis_size("tp")
    whole_value, whole_gate, whole_out = (
        lax.all_gather(w_value, "sp", axis=1, tiled=True),
        lax.all_gather(w_gate, "sp", axis=1, tiled=True),
        lax.all_gather(w_out, "sp", axis=2, tiled=True),
    )
    stream = inputs
    for layer in range(layers):
        full_rows = lax.all_gather(stream, "tp", axis=1, tiled=True)
        xf = full_rows.astype(jnp.float32)
        meansq = jnp.mean(xf * xf, axis=1, keepdims=True)
        hidden = (xf * lax.rsqrt(meansq + 1e-06) * norm_gain[layer][None, :]).astype(jnp.bfloat16)
        value = jnp.dot(hidden, whole_value[layer], preferred_element_type=jnp.float32)
        gate = jnp.dot(hidden, whole_gate[layer], preferred_element_type=jnp.float32)
        glu = (value * jax.nn.sigmoid(gate)).astype(jnp.bfloat16)
        rim = from_behind(glu[rows - reach :], "sp", 1)
        padded = jnp.concatenate([rim, glu], axis=0)
        count = padded.shape[0] - reach
        filtered = jnp.zeros((count, glu.shape[1]), jnp.float32)
        for tap in range(reach + 1):
            filtered = filtered + conv_taps[layer, tap][None, :] * padded[tap : tap + count].astype(
                jnp.float32
            )
        total_sum, total_sq = lax.psum(
            (jnp.sum(filtered, axis=1), jnp.sum(filtered * filtered, axis=1)), "tp"
        )
        mean_val = (total_sum / channels)[:, None]
        var_val = (total_sq / channels)[:, None] - mean_val * mean_val
        normed = jax.nn.silu(
            (filtered - mean_val) * lax.rsqrt(var_val + 1e-06) * ln_gain[layer][None, :]
            + ln_bias[layer][None, :]
        ).astype(jnp.bfloat16)
        partial_out = jnp.dot(normed, whole_out[layer], preferred_element_type=jnp.float32)
        summed = lax.psum_scatter(
            partial_out.astype(jnp.bfloat16), "tp", scatter_dimension=1, tiled=True
        ).astype(jnp.float32)
        kept = stream.astype(jnp.float32)
        stream = (kept + summed).astype(jnp.bfloat16)
    return stream


def solution(mesh):
    in_specs = (
        P("sp", "tp"),
        P(),
        P(None, "sp", "tp"),
        P(None, "sp", "tp"),
        P(None, None, "tp"),
        P(None, "tp"),
        P(None, "tp"),
        P(None, "tp", "sp"),
    )
    out_specs = P("sp", "tp")
    return jax.shard_map(shards, mesh=mesh, in_specs=in_specs, out_specs=out_specs, check_vma=False)
```

profile of v0, /device:TPU:0, one launch (start us, length us, event | category | flops | bytes accessed | tf_op | source)
XLA Modules:
  0.0 422.9 jit_solution(3484355526385756584)
XLA Ops:
  13.1 21.1 %all-gather.7.cloned.1.call-done = bf16[512,2048]{1,0:T(8,128)(2,1)} async-done(((bf16[512,512]{1,0:T(8,128)(2,1)}), bf16[512,2048]{1,0:T(8,128)(2,1)}) %all-gather.7.cloned.1.call-update) | async-done | bytes 2097168 | tf_op jit(solution)/shard_map/all_gather | solution.py:25
  34.2 2.1 fusion
  36.3 60.1 %all-gather.11.cloned.1.call-done = bf16[3,2048,256]{2,1,0:T(8,128)(2,1)} async-done(((bf16[3,256,256]{2,1,0:T(8,128)(2,1)}), bf16[3,2048,256]{2,1,0:T(8,128)(2,1)}) %all-gather.11.cloned.1.call-update) | async-done | bytes 3145744 | tf_op jit(solution)/shard_map/all_gather | solution.py:20
  96.4 2.8 fusion.17
  99.2 58.1 %all-gather.9.cloned.1.call-done = bf16[3,2048,256]{2,1,0:T(8,128)(2,1)} async-done(((bf16[3,256,256]{2,1,0:T(8,128)(2,1)}), bf16[3,2048,256]{2,1,0:T(8,128)(2,1)}) %all-gather.9.cloned.1.call-update) | async-done | bytes 3145744 | tf_op jit(solution)/shard_map/all_gather | solution.py:19
  157.4 2.0 fusion.18
  159.4 2.5 collective-permute-start
  163.3 2.4 fusion.134
  165.7 5.7 %all-reduce.2 = (f32[512]{0:T(512)S(1)}, f32[512]{0:T(512)S(1)}) all-reduce(f32[512]{0:T(512)S(1)} %get-tuple-element.10, f32[512]{0:T(512)S(1)} %get-tuple-element.9), channel_id=1, replica_groups=mesh['sp'=8,'tp'=4] {'tp'}, use_global_device_ids=true, to_apply=%region_4.0 | all-reduce | flops 1024 | bytes 8192 | tf_op jit(solution)/shard_map/psum | solution.py:40
  171.4 49.2 %all-gather.13.cloned.1.call-done = bf16[3,256,2048]{2,1,0:T(8,128)(2,1)} async-done(((bf16[3,256,256]{2,1,0:T(8,128)(2,1)}), bf16[3,256,2048]{2,1,0:T(8,128)(2,1)}) %all-gather.13.cloned.1.call-update) | async-done | bytes 3145744 | tf_op jit(solution)/shard_map/all_gather | solution.py:21
  220.6 3.4 convolution_convert_fusion.2
  224.1 29.5 %reduce-scatter.4.cloned.1.call-done = bf16[512,512]{1,0:T(8,128)(2,1)} async-done(((bf16[512,2048]{1,0:T(8,128)(2,1)}), bf16[512,512]{1,0:T(8,128)(2,1)}) %reduce-scatter.4.cloned.1.call-update) | async-done | bytes 524304 | tf_op jit(solution)/shard_map/reduce_scatter | solution.py:50
  253.6 2.0 add_convert_fusion.2
  255.6 22.6 %all-gather.15.cloned.1.call-done = bf16[512,2048]{1,0:T(8,128)(2,1)} async-done(((bf16[512,512]{1,0:T(8,128)(2,1)}), bf16[512,2048]{1,0:T(8,128)(2,1)}) %all-gather.15.cloned.1.call-update) | async-done | bytes 2097168 | tf_op jit(solution)/shard_map/all_gather | solution.py:25
  278.3 2.1 fusion.3
  280.4 2.8 fusion.14
  283.2 2.0 fusion.19
  285.2 3.4 collective-permute-start.1
  290.0 2.4 fusion.133
  292.4 6.0 %all-reduce.1 = (f32[512]{0:T(512)S(1)}, f32[512]{0:T(512)S(1)}) all-reduce(f32[512]{0:T(512)S(1)} %get-tuple-element.8, f32[512]{0:T(512)S(1)} %get-tuple-element.7), channel_id=1, replica_groups=mesh['sp'=8,'tp'=4] {'tp'}, use_global_device_ids=true, to_apply=%region_10.11 | all-reduce | flops 1024 | bytes 8192 | tf_op jit(solution)/shard_map/psum | solution.py:40
  298.4 3.4 convolution_convert_fusion.1
  301.9 32.1 %reduce-scatter.6.cloned.1.call-done = bf16[512,512]{1,0:T(8,128)(2,1)} async-done(((bf16[512,2048]{1,0:T(8,128)(2,1)}), bf16[512,512]{1,0:T(8,128)(2,1)}) %reduce-scatter.6.cloned.1.call-update) | async-done | bytes 524304 | tf_op jit(solution)/shard_map/reduce_scatter | solution.py:50
  334.0 2.0 add_convert_fusion.1
  336.0 22.7 %all-gather.17.cloned.1.call-done = bf16[512,2048]{1,0:T(8,128)(2,1)} async-done(((bf16[512,512]{1,0:T(8,128)(2,1)}), bf16[512,2048]{1,0:T(8,128)(2,1)}) %all-gather.17.cloned.1.call-update) | async-done | bytes 2097168 | tf_op jit(solution)/shard_map/all_gather | solution.py:25
  358.7 2.1 fusion.6
  360.8 2.8 fusion.11
  363.6 2.0 fusion.20
  365.6 3.6 collective-permute-start.2
  370.4 2.4 fusion.132
  372.8 5.9 %all-reduce = (f32[512]{0:T(512)S(1)}, f32[512]{0:T(512)S(1)}) all-reduce(f32[512]{0:T(512)S(1)} %get-tuple-element.6, f32[512]{0:T(512)S(1)} %get-tuple-element.5), channel_id=1, replica_groups=mesh['sp'=8,'tp'=4] {'tp'}, use_global_device_ids=true, to_apply=%region_16.17 | all-reduce | flops 1024 | bytes 8192 | tf_op jit(solution)/shard_map/psum | solution.py:40
  378.8 3.4 convolution_convert_fusion
  382.2 32.1 %reduce-scatter.8.cloned.1.call-done = bf16[512,512]{1,0:T(8,128)(2,1)} async-done(((bf16[512,2048]{1,0:T(8,128)(2,1)}), bf16[512,512]{1,0:T(8,128)(2,1)}) %reduce-scatter.8.cloned.1.call-update) | async-done | bytes 524304 | tf_op jit(solution)/shard_map/reduce_scatter | solution.py:50
  (55 shorter events, 12.9 us)
Async XLA Ops:
  6.5 27.7 %all-gather.7.cloned.1.call-start = ((), (), s32[]{:S(2)}) async-start(), calls=%async_computation.3 | async-start | bytes 2621440 | tf_op jit(solution)/shard_map/all_gather | solution.py:25
  7.3 89.2 %all-gather.11.cloned.1.call-start = ((), (), s32[]{:S(2)}) async-start(), calls=%async_computation.5 | async-start | bytes 3538944 | tf_op jit(solution)/shard_map/all_gather | solution.py:20
  8.0 149.3 %all-gather.9.cloned.1.call-start = ((), (), s32[]{:S(2)}) async-start(), calls=%async_computation.4 | async-start | bytes 3538944 | tf_op jit(solution)/shard_map/all_gather | solution.py:19
  8.7 211.9 %all-gather.13.cloned.1.call-start = ((), (), s32[]{:S(2)}) async-start(), calls=%async_computation.6 | async-start | bytes 3538944 | tf_op jit(solution)/shard_map/all_gather | solution.py:21
  9.3 244.2 %reduce-scatter.4.cloned.1.call-start = ((), (), s32[]{:S(2)}) async-start(), calls=%async_computation.7 | async-start | bytes 2621440 | tf_op jit(solution)/shard_map/reduce_scatter | solution.py:50
  96.4 60.9 %copy-start.3 = (bf16[512,2048]{1,0:T(8,128)(2,1)S(1)}, bf16[512,2048]{1,0:T(8,128)(2,1)}, u32[]{:S(2)}) copy-start(bf16[512,2048]{1,0:T(8,128)(2,1)} %all-gather.7.cloned.1.call-done) | copy-start | bytes 6291460
  99.2 62.6 %copy-start.7 = (f32[3,256]{1,0:T(4,128)S(1)}, f32[3,256]{1,0:T(4,128)}, u32[]{:S(2)}) copy-start(f32[3,256]{1,0:T(4,128)} %param.14) | copy-start | bytes 9220
  159.4 3.9 collective-permute-start
  220.6 33.0 %copy-start.2 = (bf16[512,512]{1,0:T(8,128)(2,1)S(1)}, bf16[512,512]{1,0:T(8,128)(2,1)}, u32[]{:S(2)}) copy-start(bf16[512,512]{1,0:T(8,128)(2,1)} %param.8) | copy-start | bytes 1572868
  224.0 31.6 %copy-start.6 = (f32[3,31,256]{2,1,0:T(8,128)S(1)}, f32[3,31,256]{2,1,0:T(8,128)}, u32[]{:S(2)}) copy-start(f32[3,31,256]{2,1,0:T(8,128)} %param.12) | copy-start | bytes 285700
  224.0 54.3 %all-gather.15.cloned.1.call-start = ((), (), s32[]{:S(2)}) async-start(), calls=%async_computation.8 | async-start | bytes 2621440 | tf_op jit(solution)/shard_map/all_gather | solution.py:25
  255.6 78.4 %reduce-scatter.6.cloned.1.call-start = ((), (), s32[]{:S(2)}) async-start(), calls=%async_computation.9 | async-start | bytes 2621440 | tf_op jit(solution)/shard_map/reduce_scatter | solution.py:50
  280.4 2.8 copy-start.4
  285.2 4.8 %collective-permute-start.1 = (bf16[30,256]{1,0:T(8,128)(2,1)S(1)}, bf16[30,256]{1,0:T(8,128)(2,1)S(1)}, u32[]{:S(2)}, u32[]{:S(2)}) collective-permute-start(bf16[30,256]{1,0:T(8,128)(2,1)S(1)} %slice.880), channel_id=1, source_target_pairs={{0,4},{4,8},{8,12},{12,16},{16,20},{20,24},{24,28},{1,5},{5,9},{9,... | collective-permute-start | bytes 46088 | tf_op jit(solution)/shard_map/ppermute | solution.py:10
  298.4 35.5 %copy-start = (bf16[512,512]{1,0:T(8,128)(2,1)S(1)}, bf16[512,512]{1,0:T(8,128)(2,1)}, u32[]{:S(2)}) copy-start(bf16[512,512]{1,0:T(8,128)(2,1)} %add_convert_fusion.2) | copy-start | bytes 1572868
  301.8 56.8 %all-gather.17.cloned.1.call-start = ((), (), s32[]{:S(2)}) async-start(), calls=%async_computation.10 | async-start | bytes 2621440 | tf_op jit(solution)/shard_map/all_gather | solution.py:25
  336.0 78.4 %reduce-scatter.8.cloned.1.call-start = ((), (), s32[]{:S(2)}) async-start(), calls=%async_computation.11 | async-start | bytes 2621440 | tf_op jit(solution)/shard_map/reduce_scatter | solution.py:50
  360.8 2.8 copy-start.5
  365.6 4.8 %collective-permute-start.2 = (bf16[30,256]{1,0:T(8,128)(2,1)S(1)}, bf16[30,256]{1,0:T(8,128)(2,1)S(1)}, u32[]{:S(2)}, u32[]{:S(2)}) collective-permute-start(bf16[30,256]{1,0:T(8,128)(2,1)S(1)} %slice.942), channel_id=1, source_target_pairs={{0,4},{4,8},{8,12},{12,16},{16,20},{20,24},{24,28},{1,5},{5,9},{9,... | collective-permute-start | bytes 46088 | tf_op jit(solution)/shard_map/ppermute | solution.py:10
  378.8 35.6 %copy-start.1 = (bf16[512,512]{1,0:T(8,128)(2,1)S(1)}, bf16[512,512]{1,0:T(8,128)(2,1)}, u32[]{:S(2)}) copy-start(bf16[512,512]{1,0:T(8,128)(2,1)} %add_convert_fusion.1) | copy-start | bytes 1572868
Sparse Core Ops, SparseCore 0:
  8.9 25.2 all-gather.6
  36.4 60.0 all-gather.10
  98.6 58.6 all-gather.8
  159.2 61.3 all-gather.12
  224.1 29.3 reduce-scatter.3
  255.7 22.5 all-gather.14
  302.0 31.9 reduce-scatter.5
  336.1 22.5 all-gather.16
  382.4 31.9 reduce-scatter.7
where the time goes:
time: 424 us; the launch traced here: 423 us
  waiting for transfers between devices  334 us (79%)
  matrix products  24.6 us (6%)
  other arithmetic  19.5 us (5%)
  blocking collectives  17.6 us (4%)
  between operations  13.4 us (3%)
  starting transfers between devices  9.7 us (2%)
    reduce_scatter x3, waiting for transfers between devices, shards(): lax.psum_scatter(partial_out.astype(jnp.bfloat16), 'tp', scatter_dimensio...  93.7 us
    all_gather x3, waiting for transfers between devices, shards(): full_rows = lax.all_gather(stream, 'tp', axis=1, tiled=True)  66.4 us
    all_gather x1, waiting for transfers between devices, shards(): lax.all_gather(w_gate, 'sp', axis=1, tiled=True)  60.1 us
    all_gather x1, waiting for transfers between devices, shards(): lax.all_gather(w_value, 'sp', axis=1, tiled=True)  58.1 us
    all_gather x1, waiting for transfers between devices, shards(): lax.all_gather(w_out, 'sp', axis=2, tiled=True)  49.2 us
    psum x3, blocking collectives, shards(): lax.psum((jnp.sum(filtered, axis=1), jnp.sum(filtered * filtered, axis=1)...  17.6 us
    dot_general x3, matrix products, shards(): jnp.dot(normed, whole_out[layer], preferred_element_type=jnp.float32)  10.2 us
    ppermute x3, starting transfers between devices, from_behind(): return lax.ppermute(block, axis, route)  9.38 us
  transfers between devices with their start and end apart: 12, of which 12 were waited for; matrix products, arithmetic and copies ran while one was open for 3% of the time, Pallas kernels for 0%

commit v1 on v0

--- a/solution.py
+++ b/solution.py
@@ -16,7 +16,9 @@
     layers = conv_taps.shape[0]
     channels = conv_taps.shape[2] * lax.axis_size("tp")
     whole_value, whole_gate, whole_out = (
-        lax.all_gather(w_value, "sp", axis=1, tiled=True),
+        jnp.concatenate(
+            lax.all_to_all(jnp.stack([w_value] * lax.axis_size("sp")), "sp", 0, 0), axis=1
+        ),
         lax.all_gather(w_gate, "sp", axis=1, tiled=True),
         lax.all_gather(w_out, "sp", axis=2, tiled=True),
     )

time: 424 us -> 392 us (0.925)
  waiting for transfers between devices: 334 us -> 296 us
  starting transfers between devices: 9.7 us -> 18 us
    all_to_all x0 -> x1, waiting for transfers between devices: none -> 79.5 us  [shards(): lax.all_to_all(jnp.stack([w_value] * lax.axis_size('sp')), 'sp', 0, 0)]
    all_gather x1 -> x0, waiting for transfers between devices: 58.1 us -> none  [shards(): lax.all_gather(w_value, 'sp', axis=1, tiled=True)]
    all_gather x1, waiting for transfers between devices: 60.1 us -> 10.2 us  [shards(): lax.all_gather(w_gate, 'sp', axis=1, tiled=True)]
    all_to_all x0 -> x1, starting transfers between devices: none -> 7.41 us  [shards(): lax.all_to_all(jnp.stack([w_value] * lax.axis_size('sp')), 'sp', 0, 0)]
    all_gather x3, waiting for transfers between devices: 66.4 us -> 60 us  [shards(): full_rows = lax.all_gather(stream, 'tp', axis=1, tiled=True)]
where the time goes in v1:
time: 392 us
  waiting for transfers between devices  296 us (76%)
  matrix products  21 us (5%)
  other arithmetic  19.5 us (5%)
  blocking collectives  18.1 us (5%)
  starting transfers between devices  18 us (5%)
  between operations  13.8 us (4%)
  local copies, waits for them, and re-layouts  5.01 us (1%)
    reduce_scatter x3, waiting for transfers between devices, shards(): lax.psum_scatter(partial_out.astype(jnp.bfloat16), 'tp', scatter_dimensio...  93.7 us
    all_to_all x1, waiting for transfers between devices, shards(): lax.all_to_all(jnp.stack([w_value] * lax.axis_size('sp')), 'sp', 0, 0)  79.5 us
    all_gather x3, waiting for transfers between devices, shards(): full_rows = lax.all_gather(stream, 'tp', axis=1, tiled=True)  60 us
    all_gather x1, waiting for transfers between devices, shards(): lax.all_gather(w_out, 'sp', axis=2, tiled=True)  46.6 us
    psum x3, blocking collectives, shards(): lax.psum((jnp.sum(filtered, axis=1), jnp.sum(filtered * filtered, axis=1)...  18.1 us
    dot_general x3, matrix products, shards(): jnp.dot(normed, whole_out[layer], preferred_element_type=jnp.float32)  10.3 us
    all_gather x1, waiting for transfers between devices, shards(): lax.all_gather(w_gate, 'sp', axis=1, tiled=True)  10.2 us
    ppermute x3, starting transfers between devices, from_behind(): return lax.ppermute(block, axis, route)  10.1 us
  transfers between devices with their start and end apart: 12, of which 12 were waited for; matrix products, arithmetic and copies ran while one was open for 3% of the time, Pallas kernels for 0%

profile of v1, /device:TPU:0, one launch (start us, length us, event | category | flops | bytes accessed | tf_op | source)
XLA Modules:
  0.0 391.7 jit_solution(11721775641366779315)
XLA Ops:
  8.0 3.0 stack.2
  11.1 7.4 %all-to-all-start = ((bf16[8,3,256,256]{3,2,1,0:T(8,128)(2,1)}), bf16[8,3,256,256]{3,2,1,0:T(8,128)(2,1)S(1)}, u32[]{:S(2)}, u32[]{:S(2)}) async-start(bf16[8,3,256,256]{3,2,1,0:T(8,128)(2,1)} %stack.2), calls=%async_computation | async-start | bytes 6291456 | tf_op jit(solution)/shard_map/all_to_all | solution.py:20
  19.4 14.8 %all-gather.6.cloned.1.call-done = bf16[512,2048]{1,0:T(8,128)(2,1)} async-done(((bf16[512,512]{1,0:T(8,128)(2,1)}), bf16[512,2048]{1,0:T(8,128)(2,1)}) %all-gather.6.cloned.1.call-update) | async-done | bytes 2097168 | tf_op jit(solution)/shard_map/all_gather | solution.py:27
  34.2 2.1 fusion
  36.3 79.5 %all-to-all-done = bf16[8,3,256,256]{3,2,1,0:T(8,128)(2,1)S(1)} async-done(((bf16[8,3,256,256]{3,2,1,0:T(8,128)(2,1)}), bf16[8,3,256,256]{3,2,1,0:T(8,128)(2,1)S(1)}, u32[]{:S(2)}, u32[]{:S(2)}) %all-to-all-start) | async-done | bytes 3145760 | tf_op jit(solution)/shard_map/all_to_all | solution.py:20
  117.5 10.2 %all-gather.8.cloned.1.call-done = bf16[3,2048,256]{2,1,0:T(8,128)(2,1)} async-done(((bf16[3,256,256]{2,1,0:T(8,128)(2,1)}), bf16[3,2048,256]{2,1,0:T(8,128)(2,1)}) %all-gather.8.cloned.1.call-update) | async-done | bytes 3145744 | tf_op jit(solution)/shard_map/all_gather | solution.py:22
  127.7 2.8 fusion.17
  131.3 3.4 collective-permute-start
  136.1 2.4 fusion.134
  138.6 6.3 %all-reduce.2 = (f32[512]{0:T(512)S(1)}, f32[512]{0:T(512)S(1)}) all-reduce(f32[512]{0:T(512)S(1)} %get-tuple-element.10, f32[512]{0:T(512)S(1)} %get-tuple-element.9), channel_id=1, replica_groups=mesh['sp'=8,'tp'=4] {'tp'}, use_global_device_ids=true, to_apply=%region_4.0 | all-reduce | flops 1024 | bytes 8192 | tf_op jit(solution)/shard_map/psum | solution.py:42
  144.8 46.6 %all-gather.10.cloned.1.call-done = bf16[3,256,2048]{2,1,0:T(8,128)(2,1)} async-done(((bf16[3,256,256]{2,1,0:T(8,128)(2,1)}), bf16[3,256,2048]{2,1,0:T(8,128)(2,1)}) %all-gather.10.cloned.1.call-update) | async-done | bytes 3145744 | tf_op jit(solution)/shard_map/all_gather | solution.py:23
  191.4 3.4 convolution_convert_fusion.2
  194.9 29.5 %reduce-scatter.4.cloned.1.call-done = bf16[512,512]{1,0:T(8,128)(2,1)} async-done(((bf16[512,2048]{1,0:T(8,128)(2,1)}), bf16[512,512]{1,0:T(8,128)(2,1)}) %reduce-scatter.4.cloned.1.call-update) | async-done | bytes 524304 | tf_op jit(solution)/shard_map/reduce_scatter | solution.py:52
  224.4 2.0 add_convert_fusion.2
  226.5 22.6 %all-gather.12.cloned.1.call-done = bf16[512,2048]{1,0:T(8,128)(2,1)} async-done(((bf16[512,512]{1,0:T(8,128)(2,1)}), bf16[512,2048]{1,0:T(8,128)(2,1)}) %all-gather.12.cloned.1.call-update) | async-done | bytes 2097168 | tf_op jit(solution)/shard_map/all_gather | solution.py:27
  249.1 2.1 fusion.3
  251.2 2.8 fusion.14
  254.8 3.4 collective-permute-start.1
  259.6 2.4 fusion.133
  262.1 5.9 %all-reduce.1 = (f32[512]{0:T(512)S(1)}, f32[512]{0:T(512)S(1)}) all-reduce(f32[512]{0:T(512)S(1)} %get-tuple-element.8, f32[512]{0:T(512)S(1)} %get-tuple-element.7), channel_id=1, replica_groups=mesh['sp'=8,'tp'=4] {'tp'}, use_global_device_ids=true, to_apply=%region_10.11 | all-reduce | flops 1024 | bytes 8192 | tf_op jit(solution)/shard_map/psum | solution.py:42
  268.0 3.4 convolution_convert_fusion.1
  271.5 32.1 %reduce-scatter.6.cloned.1.call-done = bf16[512,512]{1,0:T(8,128)(2,1)} async-done(((bf16[512,2048]{1,0:T(8,128)(2,1)}), bf16[512,512]{1,0:T(8,128)(2,1)}) %reduce-scatter.6.cloned.1.call-update) | async-done | bytes 524304 | tf_op jit(solution)/shard_map/reduce_scatter | solution.py:52
  303.6 2.0 add_convert_fusion.1
  305.8 22.5 %all-gather.14.cloned.1.call-done = bf16[512,2048]{1,0:T(8,128)(2,1)} async-done(((bf16[512,512]{1,0:T(8,128)(2,1)}), bf16[512,2048]{1,0:T(8,128)(2,1)}) %all-gather.14.cloned.1.call-update) | async-done | bytes 2097168 | tf_op jit(solution)/shard_map/all_gather | solution.py:27
  328.3 2.1 fusion.6
  330.4 2.8 fusion.11
  334.0 3.4 collective-permute-start.2
  338.8 2.4 fusion.132
  341.3 5.9 %all-reduce = (f32[512]{0:T(512)S(1)}, f32[512]{0:T(512)S(1)}) all-reduce(f32[512]{0:T(512)S(1)} %get-tuple-element.6, f32[512]{0:T(512)S(1)} %get-tuple-element.5), channel_id=1, replica_groups=mesh['sp'=8,'tp'=4] {'tp'}, use_global_device_ids=true, to_apply=%region_16.17 | all-reduce | flops 1024 | bytes 8192 | tf_op jit(solution)/shard_map/psum | solution.py:42
  347.2 3.5 convolution_convert_fusion
  350.7 32.1 %reduce-scatter.8.cloned.1.call-done = bf16[512,512]{1,0:T(8,128)(2,1)} async-done(((bf16[512,2048]{1,0:T(8,128)(2,1)}), bf16[512,512]{1,0:T(8,128)(2,1)}) %reduce-scatter.8.cloned.1.call-update) | async-done | bytes 524304 | tf_op jit(solution)/shard_map/reduce_scatter | solution.py:52
  382.8 2.0 add_convert_fusion
  (66 shorter events, 11.2 us)
Async XLA Ops:
  6.5 27.7 %all-gather.6.cloned.1.call-start = ((), (), s32[]{:S(2)}) async-start(), calls=%async_computation.4 | async-start | bytes 2621440 | tf_op jit(solution)/shard_map/all_gather | solution.py:27
  7.3 120.4 %all-gather.8.cloned.1.call-start = ((), (), s32[]{:S(2)}) async-start(), calls=%async_computation.5 | async-start | bytes 3538944 | tf_op jit(solution)/shard_map/all_gather | solution.py:22
  11.1 8.2 %copy-start.11 = (f32[3,256]{1,0:T(4,128)S(1)}, f32[3,256]{1,0:T(4,128)}, u32[]{:S(2)}) copy-start(f32[3,256]{1,0:T(4,128)} %param.13) | copy-start | bytes 9220
  11.1 8.2 %copy-start.9 = (f32[3,31,256]{2,1,0:T(8,128)S(1)}, f32[3,31,256]{2,1,0:T(8,128)}, u32[]{:S(2)}) copy-start(f32[3,31,256]{2,1,0:T(8,128)} %param.12) | copy-start | bytes 285700
  11.1 8.3 %copy-start.10 = (f32[3,2048]{1,0:T(4,128)S(1)}, f32[3,2048]{1,0:T(4,128)}, u32[]{:S(2)}) copy-start(f32[3,2048]{1,0:T(4,128)} %param.9) | copy-start | bytes 73732
  11.1 104.7 %all-to-all-start = ((bf16[8,3,256,256]{3,2,1,0:T(8,128)(2,1)}), bf16[8,3,256,256]{3,2,1,0:T(8,128)(2,1)S(1)}, u32[]{:S(2)}, u32[]{:S(2)}) async-start(bf16[8,3,256,256]{3,2,1,0:T(8,128)(2,1)} %stack.2), calls=%async_computation | async-start | bytes 6291456 | tf_op jit(solution)/shard_map/all_to_all | solution.py:20
  18.5 173.0 %all-gather.10.cloned.1.call-start = ((), (), s32[]{:S(2)}) async-start(), calls=%async_computation.6 | async-start | bytes 3538944 | tf_op jit(solution)/shard_map/all_gather | solution.py:23
  19.2 205.2 %reduce-scatter.4.cloned.1.call-start = ((), (), s32[]{:S(2)}) async-start(), calls=%async_computation.7 | async-start | bytes 2621440 | tf_op jit(solution)/shard_map/reduce_scatter | solution.py:52
  127.7 2.8 copy-start.3
  127.7 2.8 copy-start.8
  130.5 4.2 %copy-start.12 = (f32[3,256]{1,0:T(4,128)S(1)}, f32[3,256]{1,0:T(4,128)}, u32[]{:S(2)}) copy-start(f32[3,256]{1,0:T(4,128)} %param.14) | copy-start | bytes 9220
  131.3 4.8 %collective-permute-start = (bf16[30,256]{1,0:T(8,128)(2,1)S(1)}, bf16[30,256]{1,0:T(8,128)(2,1)S(1)}, u32[]{:S(2)}, u32[]{:S(2)}) collective-permute-start(bf16[30,256]{1,0:T(8,128)(2,1)S(1)} %slice.821), channel_id=1, source_target_pairs={{0,4},{4,8},{8,12},{12,16},{16,20},{20,24},{24,28},{1,5},{5,9},{9,... | collective-permute-start | bytes 46088 | tf_op jit(solution)/shard_map/ppermute | solution.py:10
  191.4 33.0 %copy-start.2 = (bf16[512,512]{1,0:T(8,128)(2,1)S(1)}, bf16[512,512]{1,0:T(8,128)(2,1)}, u32[]{:S(2)}) copy-start(bf16[512,512]{1,0:T(8,128)(2,1)} %param.8) | copy-start | bytes 1572868
  194.9 54.2 %all-gather.12.cloned.1.call-start = ((), (), s32[]{:S(2)}) async-start(), calls=%async_computation.8 | async-start | bytes 2621440 | tf_op jit(solution)/shard_map/all_gather | solution.py:27
  226.4 77.2 %reduce-scatter.6.cloned.1.call-start = ((), (), s32[]{:S(2)}) async-start(), calls=%async_computation.9 | async-start | bytes 2621440 | tf_op jit(solution)/shard_map/reduce_scatter | solution.py:52
  251.2 2.8 copy-start.4
  251.2 2.8 copy-start.7
  254.8 4.8 %collective-permute-start.1 = (bf16[30,256]{1,0:T(8,128)(2,1)S(1)}, bf16[30,256]{1,0:T(8,128)(2,1)S(1)}, u32[]{:S(2)}, u32[]{:S(2)}) collective-permute-start(bf16[30,256]{1,0:T(8,128)(2,1)S(1)} %slice.883), channel_id=1, source_target_pairs={{0,4},{4,8},{8,12},{12,16},{16,20},{20,24},{24,28},{1,5},{5,9},{9,... | collective-permute-start | bytes 46088 | tf_op jit(solution)/shard_map/ppermute | solution.py:10
  268.0 35.6 %copy-start = (bf16[512,512]{1,0:T(8,128)(2,1)S(1)}, bf16[512,512]{1,0:T(8,128)(2,1)}, u32[]{:S(2)}) copy-start(bf16[512,512]{1,0:T(8,128)(2,1)} %add_convert_fusion.2) | copy-start | bytes 1572868
  271.5 56.9 %all-gather.14.cloned.1.call-start = ((), (), s32[]{:S(2)}) async-start(), calls=%async_computation.10 | async-start | bytes 2621440 | tf_op jit(solution)/shard_map/all_gather | solution.py:27
  305.6 77.2 %reduce-scatter.8.cloned.1.call-start = ((), (), s32[]{:S(2)}) async-start(), calls=%async_computation.11 | async-start | bytes 2621440 | tf_op jit(solution)/shard_map/reduce_scatter | solution.py:52
  330.4 2.8 copy-start.5
  330.4 2.8 copy-start.6
  334.0 4.8 %collective-permute-start.2 = (bf16[30,256]{1,0:T(8,128)(2,1)S(1)}, bf16[30,256]{1,0:T(8,128)(2,1)S(1)}, u32[]{:S(2)}, u32[]{:S(2)}) collective-permute-start(bf16[30,256]{1,0:T(8,128)(2,1)S(1)} %slice.945), channel_id=1, source_target_pairs={{0,4},{4,8},{8,12},{12,16},{16,20},{20,24},{24,28},{1,5},{5,9},{9,... | collective-permute-start | bytes 46088 | tf_op jit(solution)/shard_map/ppermute | solution.py:10
  347.2 35.6 %copy-start.1 = (bf16[512,512]{1,0:T(8,128)(2,1)S(1)}, bf16[512,512]{1,0:T(8,128)(2,1)}, u32[]{:S(2)}) copy-start(bf16[512,512]{1,0:T(8,128)(2,1)} %add_convert_fusion.1) | copy-start | bytes 1572868
Sparse Core Ops, SparseCore 0:
  8.9 25.2 all-gather.5
  36.4 91.2 all-gather.7
  129.7 61.6 all-gather.9
  195.0 29.3 reduce-scatter.3
  226.5 22.5 all-gather.11
  271.6 31.9 reduce-scatter.5
  305.7 22.5 all-gather.13
  350.8 31.9 reduce-scatter.7
